TPU v7x, 32 devices: a whole 2x2x4 slice. The times are simulated.
32 devices in a mesh: sp: 4 (over z), fs: 4 (over y, x), tp: 2 (over core).
Axes of the slice: x: 2, y: 2, z: 4, core: 2. Of those that a mesh axis runs over, the one named last changes fastest.
Arguments:
- tokens: bfloat16 [4, 512, 2048], P('fs', ('sp', 'tp')), may hold values from -6 to 6
- norm_gain: float32 [2048], replicated, may hold values from 0.1 to 1.9
- gla_query_weight: bfloat16 [2048, 512], P('sp', 'tp'), may hold values from -0.125 to 0.125
- gla_key_weight: bfloat16 [2048, 512], P('sp', 'tp'), may hold values from -0.125 to 0.125
- gla_value_weight: bfloat16 [2048, 1024], P('sp', 'tp'), may hold values from -0.125 to 0.125
- decay_down: bfloat16 [2048, 32], P('sp'), may hold values from -0.125 to 0.125
- decay_up: bfloat16 [32, 512], P(None, 'tp'), may hold values from -1 to 1
- decay_bias: float32 [512], P('tp'), may hold values from 0.5 to 12
- head_gain: float32 [128], replicated, may hold values from 0.1 to 1.9
- window_query_weight: bfloat16 [2048, 1024], P('sp', 'tp'), may hold values from -3 to 3
- window_key_weight: bfloat16 [2048, 256], P('sp', 'tp'), may hold values from -3 to 3
- window_value_weight: bfloat16 [2048, 256], P('sp', 'tp'), may hold values from -0.125 to 0.125
- sink_logit: float32 [16], P('tp'), may hold values from 3 to 7
- gla_output_weight: bfloat16 [1024, 2048], P('tp', 'sp'), may hold values from -0.125 to 0.125
- window_output_weight: bfloat16 [1024, 2048], P('tp', 'sp'), may hold values from -0.125 to 0.125
Outputs:
- mixed: bfloat16 [4, 512, 2048], P('fs', ('sp', 'tp'))
All inputs are finite; a program needn't handle non-finite values.
Results may differ from a plain program's by a relative error of at most 0.013.
Values may be sent and summed in bfloat16 or wider, within the bound.
A program may use at most 64 MiB of HBM per device.

v0:
```python
import jax
import jax.numpy as jnp
from jax import lax
from jax.sharding import PartitionSpec as P

KEY_DIM = 64
VALUE_DIM = 128
SWA_HEADS = 16
KV_HEADS = 4
HEAD_DIM = 64
WINDOW = 128
SPAN = 64
EPS = 1e-06
SOFTMAX_TEMPER = 16.0
BF = jnp.bfloat16
F32 = jnp.float32


def rms_rows(values, gain):
    mean_square = jnp.mean(values * values, axis=-1, keepdims=True)
    return values * lax.rsqrt(mean_square + EPS) * gain


def quarter(weight, along):
    width = weight.shape[along] // lax.axis_size("fs")
    return lax.dynamic_slice_in_dim(weight, lax.axis_index("fs") * width, width, along)


def shared(weight, heads):
    group = SWA_HEADS // KV_HEADS
    first = lax.axis_index("fs") * heads // group
    count = max(1, heads // group)
    return lax.dynamic_slice_in_dim(weight, first * HEAD_DIM, count * HEAD_DIM, 1)


def dot(spec, a, b):
    return jnp.einsum(spec, a.astype(BF), b.astype(BF), preferred_element_type=F32)


def per_device(
    tokens,
    norm_gain,
    gla_query_weight,
    gla_key_weight,
    gla_value_weight,
    decay_down,
    decay_up,
    decay_bias,
    head_gain,
    window_query_weight,
    window_key_weight,
    window_value_weight,
    sink_logit,
    gla_output_weight,
    window_output_weight,
):
    fs, tp, sp = (lax.axis_size(n) for n in ("fs", "tp", "sp"))
    me = lax.axis_index("sp")
    heads = sink_logit.shape[0] // fs
    maps = [
        quarter(gla_value_weight, 1),
        quarter(window_query_weight, 1),
        quarter(gla_query_weight, 1),
        quarter(gla_key_weight, 1),
        shared(window_key_weight, heads),
        shared(window_value_weight, heads),
        decay_down,
    ]
    widths = [m.shape[1] for m in maps]
    w_in = lax.all_gather(jnp.concatenate(maps, 1), "sp", axis=0, tiled=True)
    w_out = lax.all_gather(
        jnp.concatenate([quarter(gla_output_weight, 0), quarter(window_output_weight, 0)], 0), "sp"
    )
    normed = rms_rows(tokens[0].astype(F32), norm_gain).astype(BF)
    normed = lax.all_gather(normed, ("fs", "tp"), axis=0, tiled=True)
    rows = normed.shape[0] // fs
    proj = jnp.dot(normed, w_in, preferred_element_type=F32).astype(BF)
    parts = []
    at = 0
    for w in widths:
        parts.append(proj[:, at : at + w])
        at += w
    gv, wq, gq, gk, wk, wv, low = parts
    up = quarter(decay_up, 1)
    logits = jnp.dot(low, up, preferred_element_type=F32) + quarter(decay_bias, 0)
    rate = jax.nn.log_sigmoid(logits) / SOFTMAX_TEMPER
    gh = gq.shape[1] // KEY_DIM
    nb = rows // SPAN
    q = gq.astype(F32).reshape(fs, nb, SPAN, gh, KEY_DIM) * KEY_DIM ** (-0.5)
    k = gk.astype(F32).reshape(fs, nb, SPAN, gh, KEY_DIM)
    v = gv.reshape(fs, nb, SPAN, gh, VALUE_DIM)
    tri = jnp.tril(jnp.ones((SPAN, SPAN), F32))
    within = jnp.cumsum(rate.reshape(fs, nb, SPAN, gh, KEY_DIM), axis=2)
    total = within[:, :, -1]
    q_dec = q * jnp.exp(within)
    k_dec = k * jnp.exp(-within)
    k_end = k * jnp.exp(total[:, :, None] - within)
    scores = dot("bnihd,bnjhd->bnhij", q_dec, k_dec)
    scores = jnp.where(tri > 0, scores, 0.0)
    local_out = dot("bnhij,bnjhe->bnihe", scores, v)
    update = dot("bnjhd,bnjhe->bnhde", k_end, v)
    state = jnp.zeros((fs, gh, KEY_DIM, VALUE_DIM), F32)
    entering = []
    for n in range(nb):
        entering.append(state)
        state = jnp.exp(total[:, n])[..., None] * state + update[:, n]
    entering = jnp.stack(entering, 1)
    span_decay = jnp.exp(jnp.sum(total, axis=1))
    packed = jnp.concatenate([state, span_decay[..., None]], -1)
    packed = lax.all_gather(packed, "sp")

    def step(position, subtotal):
        longer = packed[position, ..., -1:] * subtotal + packed[position, ..., :-1]
        return jnp.where(position < me, longer, subtotal)

    incoming = lax.fori_loop(0, sp - 1, step, jnp.zeros_like(state))
    before = jnp.cumsum(total, axis=1) - total
    entering = entering + jnp.exp(before)[..., None] * incoming[:, None]
    gla_out = local_out + dot("bnihd,bnhde->bnihe", q_dec, entering)
    gla_hidden = rms_rows(gla_out, head_gain).astype(BF).reshape(fs * rows, gh * VALUE_DIM)
    kvh = wk.shape[1] // HEAD_DIM
    per = heads // kvh
    wb = rows // WINDOW
    kv = jnp.concatenate([wk, wv], 1).reshape(fs, rows, -1)
    edge = lax.ppermute(kv[:, rows - WINDOW :], "sp", [(i, i + 1) for i in range(sp - 1)])
    band = jnp.concatenate([edge, kv], 1)
    band = jnp.stack([band[:, i * WINDOW : (i + 2) * WINDOW] for i in range(wb)], 1).reshape(
        fs, wb, 2 * WINDOW, 2, kvh, HEAD_DIM
    )
    qw = wq.reshape(fs, wb, WINDOW, kvh, per, HEAD_DIM)
    s = dot("bnqhgd,bnkhd->bnhgqk", qw, band[:, :, :, 0]) * HEAD_DIM ** (-0.5)
    distance = jnp.arange(WINDOW)[:, None] + WINDOW - jnp.arange(2 * WINDOW)[None, :]
    where = me * rows + jnp.arange(wb)[:, None, None] * WINDOW - WINDOW + jnp.arange(2 * WINDOW)
    valid = ((distance >= 0) & (distance < WINDOW))[None] & (where >= 0)
    s = jnp.where(valid[None, :, None, None], s, -1e30)
    sink = quarter(sink_logit, 0).reshape(1, 1, kvh, per, 1, 1)
    top = jnp.maximum(jnp.max(s, -1, keepdims=True), sink)
    e = jnp.exp(s - top)
    weights = (e / (jnp.sum(e, -1, keepdims=True) + jnp.exp(sink - top))).astype(BF)
    hidden = dot("bnhgqk,bnkhd->bnqhgd", weights, band[:, :, :, 1]).astype(BF)
    hidden = hidden.reshape(fs * rows, heads * HEAD_DIM)
    both = jnp.concatenate([gla_hidden, hidden], 1)
    part = jnp.einsum("rk,skn->rsn", both, w_out, preferred_element_type=F32)
    part = part.reshape(fs * rows, -1)
    mixed = lax.psum_scatter(part, ("fs", "tp"), scatter_dimension=0, tiled=True)
    return mixed.astype(BF)[None]


def solution(mesh):
    in_specs = (
        P("fs", ("sp", "tp"), None),
        P(),
        P("sp", "tp"),
        P("sp", "tp"),
        P("sp", "tp"),
        P("sp", None),
        P(None, "tp"),
        P("tp"),
        P(),
        P("sp", "tp"),
        P("sp", "tp"),
        P("sp", "tp"),
        P("tp"),
        P("tp", "sp"),
        P("tp", "sp"),
    )
    out_specs = P("fs", ("sp", "tp"), None)
    return jax.shard_map(
        per_device, mesh=mesh, in_specs=in_specs, out_specs=out_specs, check_vma=False
    )
```

profile of v0, /device:TPU:0, one launch (start us, length us, event | category | flops | bytes accessed | tf_op | source)
XLA Modules:
  0.0 219.8 jit_solution(4197163426944656206)
XLA Ops:
  6.5 0.0 copy-start
  6.5 0.9 copy.54
  7.5 1.1 constant_dynamic-slice_fusion.2
  8.6 1.1 constant_dynamic-slice_fusion.4
  9.7 1.0 constant_dynamic-slice_fusion.6
  10.7 0.0 copy-start.5
  10.7 0.0 copy-start.6
  10.7 1.1 concatenate.23
  11.8 0.0 all-gather.8.cloned.1.call-update
  11.8 0.0 all-gather.6.cloned.1.call-start
  11.9 0.2 fusion.9
  12.1 0.8 fusion.11
  12.9 0.0 all-gather.6.cloned.1.call-update
  12.9 0.0 all-gather.10.cloned.1.call-start
  13.0 1.0 constant_dynamic-slice_fusion
  14.0 0.7 pad_maximum_fusion
  14.7 0.0 all-gather.10.cloned.1.call-update
  14.7 0.0 reduce-scatter.2.cloned.1.call-start
  14.8 0.0 copy-done.5
  14.8 0.1 dynamic_slice.54
  14.9 0.1 dynamic_slice.55
  15.0 0.1 fusion.28
  15.1 54.4 %all-gather.8.cloned.1.call-done = bf16[2048,544]{1,0:T(8,128)(2,1)} async-done(((bf16[512,544]{1,0:T(8,128)(2,1)}), bf16[2048,544]{1,0:T(8,128)(2,1)}) %all-gather.8.cloned.1.call-update) | async-done | bytes 2228240 | tf_op jit(solution)/shard_map/all_gather | solution.py:70
  69.5 28.5 %all-gather.6.cloned.1.call-done = bf16[512,2048]{1,0:T(8,128)(2,1)} async-done(((bf16[64,2048]{1,0:T(8,128)(2,1)}), bf16[512,2048]{1,0:T(8,128)(2,1)}) %all-gather.6.cloned.1.call-update) | async-done | bytes 2097168 | tf_op jit(solution)/shard_map/all_gather | solution.py:75
  97.9 3.8 %convolution_convert_fusion = bf16[512,544]{0,1:T(8,128)(2,1)S(1)} fusion(bf16[512,2048]{1,0:T(8,128)(2,1)} %all-gather.6.cloned.1.call-done, bf16[2048,544]{1,0:T(8,128)(2,1)} %all-gather.8.cloned.1.call-done), kind=kOutput, calls=%fused_computation.5 | convolution fusion | flops 1141129216 | bytes 4882432 | tf_op jit(solution)/shard_map/dot_general | solution.py:77
  101.8 0.4 fusion.18
  102.2 0.1 copy.83
  102.3 0.2 fusion.38
  102.6 0.1 copy.63
  102.7 0.1 copy.85
  102.9 0.1 copy.55
  103.0 0.7 copy.100
  103.7 0.7 reshape.337
  104.4 0.1 copy.82
  104.5 4.0 %collective-permute-start = (bf16[4,128,128]{1,2,0:T(8,128)(2,1)}, bf16[4,128,128]{1,2,0:T(8,128)(2,1)}, u32[]{:S(2)}, u32[]{:S(2)}) collective-permute-start(bf16[4,128,128]{1,2,0:T(8,128)(2,1)} %bitcast.104), channel_id=1, source_target_pairs={{0,8},{8,16},{16,24},{1,9},{9,17},{17,25},{2,10},{10,18},{18,26},{... | collective-permute-start | bytes 393224 | tf_op jit(solution)/shard_map/ppermute | solution.py:125
  108.6 0.2 convolution_bitcast_fusion
  108.9 0.1 bitcast_add_fusion.2
  109.0 0.1 fusion.19
  109.1 36.6 %all-gather = f32[16,1,64,129]{3,2,1,0:T(8,128)S(1)} all-gather(f32[4,1,64,129]{3,2,1,0:T(8,128)S(1)} %maximum_bitcast_fusion), channel_id=2, replica_groups=mesh['sp'=4,'fs'=4,'tp'=2] {'sp'}, dimensions={0}, use_global_device_ids=true | all-gather | bytes 660480 | tf_op jit(solution)/shard_map/all_gather | solution.py:110
  145.7 0.9 copy.65
  146.6 0.6 while.14
  146.6 0.1 fusion.50
  146.8 0.2 fusion.50
  147.0 0.2 fusion.50
  147.2 0.0 copy-start.4
  147.2 0.1 copy.66
  147.3 0.3 fusion.6
  147.6 0.4 multiply_reduce_fusion
  148.0 0.1 multiply_convert_fusion
  148.2 0.0 collective-permute-done
  148.2 0.9 copy_dynamic-update-slice_fusion.1
  149.2 0.4 fusion.37
  149.5 0.1 broadcast_maximum_fusion
  149.6 0.2 fusion.8
  149.8 0.1 exponential_add_fusion
  149.9 0.3 fusion.5
  150.2 0.2 copy.84
  150.4 0.1 reshape.349
  150.5 0.0 all-gather.10.cloned.1.call-done
  150.5 3.9 %fusion.13 = f32[512,4,512]{0,2,1:T(8,128)} fusion(bf16[4,256,512]{2,1,0:T(8,128)(2,1)} %bitcast.124, bf16[512,128]{1,0:T(8,128)(2,1)S(1)} %reshape.349, bf16[512,128]{1,0:T(8,128)(2,1)S(1)} %bitcast.125), kind=kOutput, calls=%fused_computation.29 | convolution fusion | flops 537395200 | bytes 5505024 | tf_op jit(solution)/shard_map/rk,skn->rsn/dot_general | solution.py:143
  154.5 5.4 %copy.76 = f32[512,2048]{1,0:T(8,128)} copy(f32[512,2048]{0,1:T(8,128)} %bitcast.112) | data formatting | bytes 8388608 | tf_op jit(solution)/shard_map/reshape | solution.py:144
  159.9 0.0 reduce-scatter.2.cloned.1.call-update
  159.9 51.5 %reduce-scatter.2.cloned.1.call-done = f32[64,2048]{1,0:T(8,128)} async-done(((f32[512,2048]{1,0:T(8,128)}), f32[64,2048]{1,0:T(8,128)}) %reduce-scatter.2.cloned.1.call-update) | async-done | bytes 524304 | tf_op jit(solution)/shard_map/reduce_scatter | solution.py:145
  211.5 1.8 convert_bitcast_fusion
  (32 shorter events, 0.4 us)
Async XLA Ops:
  6.5 95.3 %copy-start = (bf16[32,256]{1,0:T(8,128)(2,1)S(1)}, bf16[32,256]{1,0:T(8,128)(2,1)}, u32[]{:S(2)}) copy-start(bf16[32,256]{1,0:T(8,128)(2,1)} %param.23) | copy-start | bytes 49156
  6.5 5.4 %copy-start.1 = (bf16[1,64,2048]{2,1,0:T(8,128)(2,1)S(1)}, bf16[1,64,2048]{2,1,0:T(8,128)(2,1)}, u32[]{:S(2)}) copy-start(bf16[1,64,2048]{2,1,0:T(8,128)(2,1)} %param.17) | copy-start | bytes 786436
  6.5 62.9 %all-gather.8.cloned.1.call-start = ((), (), s32[]{:S(2)}) async-start(), calls=%async_computation.2 | async-start | bytes 3276800 | tf_op jit(solution)/shard_map/all_gather | solution.py:70
  6.5 5.5 %copy-start.3 = (f32[2048]{0:T(1024)S(1)}, f32[2048]{0:T(1024)}, u32[]{:S(2)}) copy-start(f32[2048]{0:T(1024)} %param.18) | copy-start | bytes 24580
  10.7 4.1 %copy-start.5 = (f32[256]{0:T(256)S(1)}, f32[256]{0:T(256)}, u32[]{:S(2)}) copy-start(f32[256]{0:T(256)} %param.24) | copy-start | bytes 3076
  10.7 4.2 %copy-start.6 = (f32[8]{0:T(128)S(1)}, f32[8]{0:T(128)}, u32[]{:S(2)}) copy-start(f32[8]{0:T(128)} %param.29) | copy-start | bytes 100
  11.8 86.1 %all-gather.6.cloned.1.call-start = ((), (), s32[]{:S(2)}) async-start(), calls=%async_computation.1 | async-start | bytes 2359296 | tf_op jit(solution)/shard_map/all_gather | solution.py:75
  12.9 137.6 %all-gather.10.cloned.1.call-start = ((), (), s32[]{:S(2)}) async-start(), calls=%async_computation.4 | async-start | bytes 1310720 | tf_op jit(solution)/shard_map/all_gather | solution.py:71
  14.7 196.8 %reduce-scatter.2.cloned.1.call-start = ((), (), s32[]{:S(2)}) async-start(), calls=%async_computation.3 | async-start | bytes 4718592 | tf_op jit(solution)/shard_map/reduce_scatter | solution.py:145
  104.5 43.7 %collective-permute-start = (bf16[4,128,128]{1,2,0:T(8,128)(2,1)}, bf16[4,128,128]{1,2,0:T(8,128)(2,1)}, u32[]{:S(2)}, u32[]{:S(2)}) collective-permute-start(bf16[4,128,128]{1,2,0:T(8,128)(2,1)} %bitcast.104), channel_id=1, source_target_pairs={{0,8},{8,16},{16,24},{1,9},{9,17},{17,25},{2,10},{10,18},{18,26},{... | collective-permute-start | bytes 393224 | tf_op jit(solution)/shard_map/ppermute | solution.py:125
  147.2 0.9 copy-start.4
  147.2 2.0 copy-start.2
Sparse Core Ops, SparseCore 0:
  12.0 57.4 all-gather.7
  71.4 26.5 all-gather.5
  99.5 42.4 all-gather.9
  160.1 51.3 reduce-scatter.1
where the time goes:
time: 220 us
  waiting for transfers between devices  134 us (61%)
  blocking collectives  36.6 us (17%)
  local copies, waits for them, and re-layouts  16.2 us (7%)
  between operations  13.5 us (6%)
  matrix products  9.71 us (4%)
  other arithmetic  5.13 us (2%)
  starting transfers between devices  4.18 us (2%)
    all_gather x1, waiting for transfers between devices, per_device(): w_in = lax.all_gather(jnp.concatenate(maps, 1), 'sp', axis=0, tiled=True)  54.4 us
    reduce_scatter x1, waiting for transfers between devices, per_device(): lax.psum_scatter(part, ('fs', 'tp'), scatter_dimension=0, tiled=True)  51.5 us
    all_gather x1, blocking collectives, per_device(): packed = lax.all_gather(packed, 'sp')  36.6 us
    all_gather x1, waiting for transfers between devices, per_device(): normed = lax.all_gather(normed, ('fs', 'tp'), axis=0, tiled=True)  28.5 us
    reshape x1, local copies, waits for them, and re-layouts, per_device(): part = part.reshape(fs * rows, -1)  5.43 us
  transfers between devices with their start and end apart: 5, of which 3 were waited for; matrix products, arithmetic and copies ran while one was open for 7% of the time, Pallas kernels for 0%

commit v1 on v0

--- a/solution.py
+++ b/solution.py
@@ -72,7 +72,10 @@
         jnp.concatenate([quarter(gla_output_weight, 0), quarter(window_output_weight, 0)], 0), "sp"
     )
     normed = rms_rows(tokens[0].astype(F32), norm_gain).astype(BF)
-    normed = lax.all_gather(normed, ("fs", "tp"), axis=0, tiled=True)
+    size = lax.axis_size(("fs", "tp"))
+    blocks = jnp.stack([normed for _ in range(size)])
+    blocks = lax.all_to_all(blocks, ("fs", "tp"), split_axis=0, concat_axis=0)
+    normed = jnp.concatenate(blocks, axis=0)
     rows = normed.shape[0] // fs
     proj = jnp.dot(normed, w_in, preferred_element_type=F32).astype(BF)
     parts = []

time: 220 us -> 190 us (0.86)
  waiting for transfers between devices: 134 us -> 99.8 us
  starting transfers between devices: 4.18 us -> 7.76 us
    all_gather x1, waiting for transfers between devices: 54.4 us -> 23.8 us  [per_device(): w_in = lax.all_gather(jnp.concatenate(maps, 1), 'sp', axis=0, tiled=True)]
    all_gather x1 -> x0, waiting for transfers between devices: 28.5 us -> none  [per_device(): normed = lax.all_gather(normed, ('fs', 'tp'), axis=0, tiled=True)]
    all_to_all x0 -> x1, waiting for transfers between devices: none -> 24.5 us  [per_device(): blocks = lax.all_to_all(blocks, ('fs', 'tp'), split_axis=0, concat_axis=0)]
    all_to_all x0 -> x1, starting transfers between devices: none -> 5.33 us  [per_device(): blocks = lax.all_to_all(blocks, ('fs', 'tp'), split_axis=0, concat_axis=0)]
  transfers between devices with their start and end apart: 5 -> 5, of which waited for: 3 -> 3; matrix products, arithmetic and copies ran while one was open for 7% -> 8% of each run, Pallas kernels for 0% -> 0%
where the time goes in v1:
time: 190 us; the launch traced here: 189 us
  waiting for transfers between devices  99.8 us (53%)
  blocking collectives  36.8 us (19%)
  local copies, waits for them, and re-layouts  17.8 us (9%)
  between operations  13.4 us (7%)
  matrix products  9.1 us (5%)
  starting transfers between devices  7.76 us (4%)
  other arithmetic  4.41 us (2%)
    reduce_scatter x1, waiting for transfers between devices, per_device(): lax.psum_scatter(part, ('fs', 'tp'), scatter_dimension=0, tiled=True)  51.5 us
    all_gather x1, blocking collectives, per_device(): packed = lax.all_gather(packed, 'sp')  36.8 us
    all_to_all x1, waiting for transfers between devices, per_device(): blocks = lax.all_to_all(blocks, ('fs', 'tp'), split_axis=0, concat_axis=0)  24.5 us
    all_gather x1, waiting for transfers between devices, per_device(): w_in = lax.all_gather(jnp.concatenate(maps, 1), 'sp', axis=0, tiled=True)  23.8 us
    reshape x1, local copies, waits for them, and re-layouts, per_device(): part = part.reshape(fs * rows, -1)  5.41 us
    all_to_all x1, starting transfers between devices, per_device(): blocks = lax.all_to_all(blocks, ('fs', 'tp'), split_axis=0, concat_axis=0)  5.33 us
    dot_general x1, matrix products, per_device(): part = jnp.einsum('rk,skn->rsn', both, w_out, preferred_element_type=F32)  3.93 us
  transfers between devices with their start and end apart: 5, of which 3 were waited for; matrix products, arithmetic and copies ran while one was open for 8% of the time, Pallas kernels for 0%

profile of v1, /device:TPU:0, one launch (start us, length us, event | category | flops | bytes accessed | tf_op | source)
XLA Modules:
  0.0 189.1 jit_solution(8577677740357880727)
XLA Ops:
  6.5 0.0 copy-start
  6.5 0.0 all-gather.5.cloned.1.call-start
  6.5 0.9 copy.54
  7.5 1.1 constant_dynamic-slice_fusion.2
  8.6 1.1 constant_dynamic-slice_fusion.4
  9.7 1.0 constant_dynamic-slice_fusion.6
  10.7 1.1 concatenate.23
  11.8 0.0 all-gather.5.cloned.1.call-update
  11.8 0.2 fusion.9
  12.0 0.0 copy-done.3
  12.0 0.1 fusion.13
  12.1 1.6 stack.7
  13.7 5.3 %all-to-all-start = ((bf16[8,64,2048]{2,1,0:T(8,128)(2,1)}), bf16[8,64,2048]{2,1,0:T(8,128)(2,1)S(1)}, u32[]{:S(2)}, u32[]{:S(2)}) async-start(bf16[8,64,2048]{2,1,0:T(8,128)(2,1)} %stack.7), calls=%async_computation | async-start | bytes 4194304 | tf_op jit(solution)/shard_map/all_to_all | solution.py:77
  19.1 0.0 all-gather.7.cloned.1.call-start
  19.1 1.0 constant_dynamic-slice_fusion
  20.1 0.7 pad_maximum_fusion
  20.8 0.0 all-gather.7.cloned.1.call-update
  20.8 0.0 reduce-scatter.2.cloned.1.call-start
  20.9 0.1 dynamic_slice.54
  21.0 0.1 dynamic_slice.55
  21.1 0.1 fusion.29
  21.2 24.5 %all-to-all-done = bf16[8,64,2048]{2,1,0:T(8,128)(2,1)S(1)} async-done(((bf16[8,64,2048]{2,1,0:T(8,128)(2,1)}), bf16[8,64,2048]{2,1,0:T(8,128)(2,1)S(1)}, u32[]{:S(2)}, u32[]{:S(2)}) %all-to-all-start) | async-done | bytes 2097184 | tf_op jit(solution)/shard_map/all_to_all | solution.py:77
  45.7 23.8 %all-gather.5.cloned.1.call-done = bf16[2048,544]{1,0:T(8,128)(2,1)} async-done(((bf16[512,544]{1,0:T(8,128)(2,1)}), bf16[2048,544]{1,0:T(8,128)(2,1)}) %all-gather.5.cloned.1.call-update) | async-done | bytes 2228240 | tf_op jit(solution)/shard_map/all_gather | solution.py:70
  69.4 3.2 %convolution_convert_fusion = bf16[512,544]{0,1:T(8,128)(2,1)S(1)} fusion(bf16[512,2048]{1,0:T(8,128)(2,1)S(1)} %bitcast.119, bf16[2048,544]{1,0:T(8,128)(2,1)} %all-gather.5.cloned.1.call-done), kind=kOutput, calls=%fused_computation.5 | convolution fusion | flops 1141129216 | bytes 4882432 | tf_op jit(solution)/shard_map/dot_general | solution.py:80
  72.7 0.4 fusion.19
  73.1 0.1 copy.83
  73.2 0.2 fusion.39
  73.5 0.1 copy.63
  73.6 0.1 copy.85
  73.8 0.1 copy.55
  73.9 0.7 copy.100
  74.6 0.7 reshape.355
  75.3 0.1 copy.82
  75.4 2.3 %collective-permute-start = (bf16[4,128,128]{1,2,0:T(8,128)(2,1)}, bf16[4,128,128]{1,2,0:T(8,128)(2,1)}, u32[]{:S(2)}, u32[]{:S(2)}) collective-permute-start(bf16[4,128,128]{1,2,0:T(8,128)(2,1)} %bitcast.103), channel_id=1, source_target_pairs={{0,8},{8,16},{16,24},{1,9},{9,17},{17,25},{2,10},{10,18},{18,26},{... | collective-permute-start | bytes 393224 | tf_op jit(solution)/shard_map/ppermute | solution.py:128
  77.8 0.2 convolution_bitcast_fusion
  78.1 0.1 bitcast_add_fusion.2
  78.2 0.1 fusion.20
  78.3 36.8 %all-gather = f32[16,1,64,129]{3,2,1,0:T(8,128)S(1)} all-gather(f32[4,1,64,129]{3,2,1,0:T(8,128)S(1)} %maximum_bitcast_fusion), channel_id=2, replica_groups=mesh['sp'=4,'fs'=4,'tp'=2] {'sp'}, dimensions={0}, use_global_device_ids=true | all-gather | bytes 660480 | tf_op jit(solution)/shard_map/all_gather | solution.py:113
  115.2 0.9 copy.65
  116.1 0.5 while.14
  116.1 0.1 fusion.51
  116.3 0.1 fusion.51
  116.4 0.1 fusion.51
  116.6 0.0 copy-start.4
  116.6 0.1 copy.66
  116.7 0.3 fusion.6
  117.1 0.4 multiply_reduce_fusion
  117.5 0.0 copy-done.4
  117.5 0.1 multiply_convert_fusion
  117.6 0.0 collective-permute-done
  117.6 0.9 copy_dynamic-update-slice_fusion.1
  118.6 0.4 fusion.38
  119.0 0.1 broadcast_maximum_fusion
  119.1 0.2 fusion.8
  119.2 0.1 exponential_add_fusion
  119.3 0.3 fusion.5
  119.6 0.2 copy.84
  119.8 0.1 reshape.366
  120.0 0.0 all-gather.7.cloned.1.call-done
  120.0 3.9 %fusion.14 = f32[512,4,512]{0,2,1:T(8,128)} fusion(bf16[4,256,512]{2,1,0:T(8,128)(2,1)} %bitcast.124, bf16[512,128]{1,0:T(8,128)(2,1)S(1)} %reshape.366, bf16[512,128]{1,0:T(8,128)(2,1)S(1)} %bitcast.125), kind=kOutput, calls=%fused_computation.30 | convolution fusion | flops 537395200 | bytes 5505024 | tf_op jit(solution)/shard_map/rk,skn->rsn/dot_general | solution.py:146
  123.9 5.4 %copy.76 = f32[512,2048]{1,0:T(8,128)} copy(f32[512,2048]{0,1:T(8,128)} %bitcast.111) | data formatting | bytes 8388608 | tf_op jit(solution)/shard_map/reshape | solution.py:147
  129.3 0.0 reduce-scatter.2.cloned.1.call-update
  129.3 51.5 %reduce-scatter.2.cloned.1.call-done = f32[64,2048]{1,0:T(8,128)} async-done(((f32[512,2048]{1,0:T(8,128)}), f32[64,2048]{1,0:T(8,128)}) %reduce-scatter.2.cloned.1.call-update) | async-done | bytes 524304 | tf_op jit(solution)/shard_map/reduce_scatter | solution.py:148
  180.8 1.8 convert_bitcast_fusion
  (32 shorter events, 0.4 us)
Async XLA Ops:
  6.5 66.2 %copy-start = (bf16[32,256]{1,0:T(8,128)(2,1)S(1)}, bf16[32,256]{1,0:T(8,128)(2,1)}, u32[]{:S(2)}) copy-start(bf16[32,256]{1,0:T(8,128)(2,1)} %param.23) | copy-start | bytes 49156
  6.5 5.3 %copy-start.1 = (bf16[1,64,2048]{2,1,0:T(8,128)(2,1)S(1)}, bf16[1,64,2048]{2,1,0:T(8,128)(2,1)}, u32[]{:S(2)}) copy-start(bf16[1,64,2048]{2,1,0:T(8,128)(2,1)} %param.17) | copy-start | bytes 786436
  6.5 62.9 %all-gather.5.cloned.1.call-start = ((), (), s32[]{:S(2)}) async-start(), calls=%async_computation.2 | async-start | bytes 3276800 | tf_op jit(solution)/shard_map/all_gather | solution.py:70
  6.5 5.4 %copy-start.3 = (f32[2048]{0:T(1024)S(1)}, f32[2048]{0:T(1024)}, u32[]{:S(2)}) copy-start(f32[2048]{0:T(1024)} %param.18) | copy-start | bytes 24580
  13.7 7.2 %copy-start.5 = (f32[256]{0:T(256)S(1)}, f32[256]{0:T(256)}, u32[]{:S(2)}) copy-start(f32[256]{0:T(256)} %param.24) | copy-start | bytes 3076
  13.7 7.3 %copy-start.6 = (f32[8]{0:T(128)S(1)}, f32[8]{0:T(128)}, u32[]{:S(2)}) copy-start(f32[8]{0:T(128)} %param.29) | copy-start | bytes 100
  13.7 31.9 %all-to-all-start = ((bf16[8,64,2048]{2,1,0:T(8,128)(2,1)}), bf16[8,64,2048]{2,1,0:T(8,128)(2,1)S(1)}, u32[]{:S(2)}, u32[]{:S(2)}) async-start(bf16[8,64,2048]{2,1,0:T(8,128)(2,1)} %stack.7), calls=%async_computation | async-start | bytes 4194304 | tf_op jit(solution)/shard_map/all_to_all | solution.py:77
  19.1 100.9 %all-gather.7.cloned.1.call-start = ((), (), s32[]{:S(2)}) async-start(), calls=%async_computation.4 | async-start | bytes 1310720 | tf_op jit(solution)/shard_map/all_gather | solution.py:71
  20.8 160.0 %reduce-scatter.2.cloned.1.call-start = ((), (), s32[]{:S(2)}) async-start(), calls=%async_computation.3 | async-start | bytes 4718592 | tf_op jit(solution)/shard_map/reduce_scatter | solution.py:148
  75.4 42.2 %collective-permute-start = (bf16[4,128,128]{1,2,0:T(8,128)(2,1)}, bf16[4,128,128]{1,2,0:T(8,128)(2,1)}, u32[]{:S(2)}, u32[]{:S(2)}) collective-permute-start(bf16[4,128,128]{1,2,0:T(8,128)(2,1)} %bitcast.103), channel_id=1, source_target_pairs={{0,8},{8,16},{16,24},{1,9},{9,17},{17,25},{2,10},{10,18},{18,26},{... | collective-permute-start | bytes 393224 | tf_op jit(solution)/shard_map/ppermute | solution.py:128
  116.6 0.9 copy-start.4
  116.6 2.0 %copy-start.2 = (bf16[4,128,2,64]{1,0,3,2:T(4,128)(2,1)S(1)}, bf16[4,128,2,64]{1,0,3,2:T(4,128)(2,1)}, u32[]{:S(2)}) copy-start(bf16[4,128,2,64]{1,0,3,2:T(4,128)(2,1)} %reshape.355) | copy-start | bytes 393220
Sparse Core Ops, SparseCore 0:
  11.9 57.4 all-gather.4
  71.0 42.8 all-gather.6
  129.5 51.3 reduce-scatter.1
